TPU v7x, 32 devices: a whole 2x2x4 slice. The times are simulated.
32 devices in a mesh: sp: 8 (over z, y), tp: 4 (over x, core).
Axes of the slice: x: 2, y: 2, z: 4, core: 2. Of those that a mesh axis runs over, the one named last changes fastest.
Arguments:
- tokens: bfloat16 [1024, 2048], P('sp', 'tp'), may hold values from -28 to 28
- norm_gain: bfloat16 [1, 2048], P(None, 'tp'), may hold values from 0.099609375 to 1.8984375
- conv_b_w: bfloat16 [2048, 1024], P(None, 'tp'), may hold values from -0.125 to 0.125
- conv_c_w: bfloat16 [2048, 1024], P(None, 'tp'), may hold values from -0.125 to 0.125
- conv_u_w: bfloat16 [2048, 1024], P(None, 'tp'), may hold values from -0.125 to 0.125
- conv_taps: bfloat16 [3, 1024], P(None, 'tp'), may hold values from -3.5 to 3.5
- query_w: bfloat16 [2048, 2048], P(None, 'tp'), may hold values from -0.125 to 0.125
- key_w: bfloat16 [2048, 2048], P(None, 'tp'), may hold values from -0.125 to 0.125
- value_w: bfloat16 [2048, 2048], P(None, 'tp'), may hold values from -0.125 to 0.125
- outgate_w: bfloat16 [2048, 2048], P(None, 'tp'), may hold values from -0.125 to 0.125
- gate_w: bfloat16 [2048, 2, 8], P(None, None, 'tp'), may hold values from -0.125 to 0.125
- gate_bias: float32 [2, 8], P(None, 'tp'), may hold values from -5 to 150
- mem_gain: bfloat16 [2048], P('tp'), may hold values from 0.099609375 to 1.8984375
- conv_out_w: bfloat16 [1024, 2048], P('tp'), may hold values from -0.1875 to 0.1875
- mem_out_w: bfloat16 [2048, 2048], P('tp'), may hold values from -0.125 to 0.125
Outputs:
- layer_out: bfloat16 [1024, 2048], P(('sp', 'tp'))
All inputs are finite; a program needn't handle non-finite values.
Results may differ from a plain program's by a relative error of at most 0.014.
The roundings to bfloat16 on the way count: a program that leaves them out, or rounds other values in their place, can miss the bound.
Values may be sent and summed in bfloat16 or wider, within the bound.
A program may use at most 64 MiB of HBM per device.

v0:
```python
import jax
import jax.numpy as jnp
from jax import lax
from jax.sharding import PartitionSpec as P

HEAD_DIM = 256
BLOCK = 128
MDIM = 2048
EPS = 1e-06
LOWEST = -1e30
HIGH = lax.Precision.HIGHEST


def shifted(value, axis, by):
    count = lax.axis_size(axis)
    pairs = [(i, i + by) for i in range(count) if 0 <= i + by < count]
    return lax.ppermute(value, axis, pairs)


def prefix(value, axis, join, neutral):
    count, mine = (lax.axis_size(axis), lax.axis_index(axis))
    pieces = jax.tree.map(lambda part: lax.all_gather(part, axis), value)
    total = jax.tree.map(
        lambda part, zero: jnp.full_like(part, 0) + jnp.asarray(zero, part.dtype), value, neutral
    )

    def prefix_step(position, total):
        longer = join(total, jax.tree.map(lambda part: part[position], pieces))
        return jax.tree.map(lambda new, old: jnp.where(position < mine, new, old), longer, total)

    return lax.fori_loop(0, count - 1, prefix_step, total)


def local_pass(queries, keys, values, input_pre, log_forget):
    count, width = queries.shape
    blocks = count // BLOCK

    def local_step(carry, inputs):
        memory, normer, stabil, decay_sum = carry
        query_block, key_block, value_block, input_gate, forget_block = inputs
        causal = jnp.tril(jnp.ones((BLOCK, BLOCK), dtype=bool))
        running = jnp.cumsum(forget_block)
        decays = jnp.where(
            causal, running[:, None] - running[None, :] + input_gate[None, :], -jnp.inf
        )
        inter = running + stabil
        row_max = jnp.maximum(inter, jnp.max(decays, axis=1))
        weights = jnp.exp(decays - row_max[:, None])
        scores = jnp.dot(query_block, key_block.T, precision=HIGH) * weights
        carried = jnp.exp(inter - row_max)
        numer_part = carried[:, None] * jnp.dot(query_block, memory, precision=HIGH) + jnp.dot(
            scores, value_block, precision=HIGH
        )
        denom_part = carried * jnp.dot(query_block, normer, precision=HIGH) + jnp.sum(
            scores, axis=1
        )
        new_stabil = row_max[-1]
        key_weight = jnp.exp(running[-1] - running + input_gate - new_stabil)
        fade = jnp.exp(running[-1] + stabil - new_stabil)
        memory = fade * memory + jnp.dot(
            (key_weight[:, None] * key_block).T, value_block, precision=HIGH
        )
        normer = fade * normer + jnp.dot(key_weight, key_block, precision=HIGH)
        outputs = (numer_part, denom_part, row_max, decay_sum + running)
        return ((memory, normer, new_stabil, decay_sum + running[-1]), outputs)

    inputs = (
        queries.reshape(blocks, BLOCK, width),
        keys.reshape(blocks, BLOCK, width),
        values.reshape(blocks, BLOCK, width),
        input_pre.reshape(blocks, BLOCK),
        log_forget.reshape(blocks, BLOCK),
    )
    start = (
        jnp.zeros((width, width), jnp.float32),
        jnp.zeros((width,), jnp.float32),
        jnp.zeros((), jnp.float32),
        jnp.zeros((), jnp.float32),
    )
    final, rows = lax.scan(local_step, start, inputs)
    memory, normer, stabil, decay_sum = final
    numer_rows, denom_rows, row_max, row_decay = rows
    return (
        numer_rows.reshape(count, width),
        denom_rows.reshape(count),
        row_max.reshape(count),
        row_decay.reshape(count),
        decay_sum,
        stabil,
        memory,
        normer,
    )


def finish(queries, numer_rows, denom_rows, row_max, row_decay, stabil_in, memory_in, normer_in):
    from_before = jnp.dot(queries, memory_in, precision=HIGH)
    normer_before = jnp.dot(queries, normer_in, precision=HIGH)
    top = jnp.maximum(row_max, row_decay + stabil_in)
    own_scale = jnp.exp(row_max - top)
    past_scale = jnp.exp(row_decay + stabil_in - top)
    numer_all = own_scale[:, None] * numer_rows + past_scale[:, None] * from_before
    denom_all = own_scale * denom_rows + past_scale * normer_before
    return numer_all / jnp.maximum(jnp.abs(denom_all), jnp.exp(-top))[:, None]


def join_state(earlier, later):
    sum_early, stab_early, mem_early, norm_early = earlier[:4]
    sum_late, stab_late, mem_late, norm_late = later[:4]
    top = jnp.maximum(sum_late + stab_early, stab_late)
    early_scale = jnp.exp(sum_late + stab_early - top)
    late_scale = jnp.exp(stab_late - top)
    joined = (
        sum_early + sum_late,
        top,
        early_scale[:, None, None] * mem_early + late_scale[:, None, None] * mem_late,
        early_scale[:, None] * norm_early + late_scale[:, None] * norm_late,
    )
    if len(earlier) > 4:
        edge = jnp.where(later[5][0] > 0, later[4], earlier[4])
        joined = joined + (edge, jnp.maximum(earlier[5], later[5]))
    return joined


def body(
    tokens,
    norm_gain,
    conv_b_w,
    conv_c_w,
    conv_u_w,
    conv_taps,
    query_w,
    key_w,
    value_w,
    outgate_w,
    gate_w,
    gate_bias,
    mem_gain,
    conv_out_w,
    mem_out_w,
):
    count = tokens.shape[0]
    model = conv_b_w.shape[0]
    weights = (
        conv_b_w,
        conv_c_w,
        conv_u_w,
        query_w,
        key_w,
        value_w,
        outgate_w,
        gate_w.reshape(model, -1),
    )
    piece = lax.all_gather(tokens, "tp", axis=1, tiled=True)
    gain_piece = lax.all_gather(norm_gain, "tp", axis=1, tiled=True)
    wide = piece.astype(jnp.float32)
    scaled = (wide * gain_piece.astype(jnp.float32)).astype(jnp.bfloat16)
    squares = jnp.sum(wide * wide, axis=1)
    totals = tuple(
        (jnp.dot(scaled, weight, preferred_element_type=jnp.float32) for weight in weights)
    )
    folded = (squares,) + totals
    inv_rms = lax.rsqrt(folded[0] / model + EPS)[:, None]

    def project(total):
        return lax.optimization_barrier((inv_rms * total).astype(jnp.bfloat16)).astype(jnp.float32)

    gate_b, gate_c, gate_u, queries, keys, values, outgate = [
        project(total) for total in folded[1:8]
    ]
    heads = gate_bias.shape[1]
    gates = inv_rms * folded[8]
    input_pre = gates[:, :heads] + gate_bias[0]
    forget_pre = gates[:, heads:] + gate_bias[1]
    mixed_in = (gate_c * gate_u).astype(jnp.bfloat16)
    reach = conv_taps.shape[0] - 1
    head_q = queries.reshape(count, heads, HEAD_DIM)
    head_k = keys.reshape(count, heads, HEAD_DIM) * HEAD_DIM ** (-0.5)
    head_v = values.reshape(count, heads, HEAD_DIM)
    local = jax.vmap(local_pass, in_axes=1, out_axes=(1, 1, 1, 1, 0, 0, 0, 0))(
        head_q, head_k, head_v, input_pre, jax.nn.log_sigmoid(forget_pre)
    )
    numer_rows, denom_rows, row_max, row_decay, decay_sum, stabil, memory, normer = local
    identity = (
        jnp.zeros((heads,), jnp.float32),
        jnp.full((heads,), LOWEST, jnp.float32),
        jnp.zeros((heads, HEAD_DIM, HEAD_DIM), jnp.float32),
        jnp.zeros((heads, HEAD_DIM), jnp.float32),
    )
    before = shifted(mixed_in[count - reach :], "sp", 1)
    incoming = prefix((decay_sum, stabil, memory, normer), "sp", join_state, identity)
    padded = jnp.concatenate([before, mixed_in], axis=0).astype(jnp.float32)
    taps = conv_taps.astype(jnp.float32)
    conv_sum = taps[0] * padded[0:count]
    for offset in range(1, reach + 1):
        conv_sum = conv_sum + taps[offset] * padded[offset : offset + count]
    y_conv = (gate_b * conv_sum).astype(jnp.bfloat16)
    mem_raw = jax.vmap(finish, in_axes=(1, 1, 1, 1, 1, 0, 0, 0), out_axes=1)(
        head_q, numer_rows, denom_rows, row_max, row_decay, incoming[1], incoming[2], incoming[3]
    )
    flat_raw = mem_raw.reshape(count, -1)
    own_squares = jnp.sum(flat_raw * flat_raw, axis=1)
    all_squares = lax.psum(own_squares, "tp")
    mem_norm = flat_raw * lax.rsqrt(all_squares / MDIM + EPS)[:, None]
    mem_norm = mem_norm * mem_gain.astype(jnp.float32)[None, :]
    y_mem = (jax.nn.sigmoid(outgate) * mem_norm).astype(jnp.bfloat16)
    return lax.psum_scatter(
        (
            jnp.dot(y_conv, conv_out_w, preferred_element_type=jnp.float32)
            + jnp.dot(y_mem, mem_out_w, preferred_element_type=jnp.float32)
        ).astype(jnp.bfloat16),
        "tp",
        scatter_dimension=0,
        tiled=True,
    )


def solution(mesh):
    return jax.shard_map(
        body,
        mesh=mesh,
        in_specs=(
            P("sp", "tp"),
            P(None, "tp"),
            P(None, "tp"),
            P(None, "tp"),
            P(None, "tp"),
            P(None, "tp"),
            P(None, "tp"),
            P(None, "tp"),
            P(None, "tp"),
            P(None, "tp"),
            P(None, None, "tp"),
            P(None, "tp"),
            P("tp"),
            P("tp", None),
            P("tp", None),
        ),
        out_specs=P(("sp", "tp"), None),
        check_vma=False,
    )
```

profile of v0, /device:TPU:0, one launch (start us, length us, event | category | flops | bytes accessed | tf_op | source)
XLA Modules:
  0.0 148.9 jit_solution(2480114630991469454)
XLA Ops:
  6.6 0.8 slice_bitcast_fusion
  7.4 6.3 %all_gather.31 = bf16[1,2048]{1,0:T(2,128)(2,1)S(1)} all-gather(bf16[1,512]{1,0:T(2,128)(2,1)} %param.18), channel_id=1, replica_groups=mesh['sp'=8,'tp'=4] {'tp'}, dimensions={1}, use_global_device_ids=true | all-gather | bytes 5120 | tf_op jit(solution)/shard_map/all_gather | solution.py:154
  14.5 7.9 %all_gather.30 = bf16[128,2048]{1,0:T(8,128)(2,1)S(1)} all-gather(bf16[128,512]{1,0:T(8,128)(2,1)} %param.17), channel_id=1, replica_groups=mesh['sp'=8,'tp'=4] {'tp'}, dimensions={1}, use_global_device_ids=true | all-gather | bytes 655360 | tf_op jit(solution)/shard_map/all_gather | solution.py:153
  23.7 2.2 %fusion.15 = bf16[128,512]{1,0:T(8,128)(2,1)S(1)} fusion(bf16[2048,512]{1,0:T(8,128)(2,1)} %param.24, f32[128]{0:T(128)S(1)} %add_rsqrt_fusion.1, bf16[128,2048]{1,0:T(8,128)(2,1)S(1)} %all_gather.30, f32[2048]{0:T(1024)S(1)} %bitcast.213), kind=kOutput, calls=%fused_computation.34 | convolution fusion | flops 269352960 | bytes 2761216 | tf_op jit(solution)/shard_map/dot_general | solution.py:159
  26.4 1.3 convolution_add_fusion.1
  27.7 1.5 %fusion.19 = bf16[128,256]{1,0:T(8,128)(2,1)S(1)} fusion(bf16[2048,256]{1,0:T(8,128)(2,1)} %param.20, f32[128]{0:T(128)S(1)} %add_rsqrt_fusion.1, bf16[128,2048]{1,0:T(8,128)(2,1)S(1)} %all_gather.30, f32[2048]{0:T(1024)S(1)} %bitcast.215), kind=kOutput, calls=%fused_computation.42 | convolution fusion | flops 135069696 | bytes 1647104 | tf_op jit(solution)/shard_map/dot_general | solution.py:159
  29.3 1.5 %fusion.20 = bf16[128,256]{1,0:T(8,128)(2,1)S(1)} fusion(bf16[2048,256]{1,0:T(8,128)(2,1)} %param.21, f32[128]{0:T(128)S(1)} %add_rsqrt_fusion.1, bf16[128,2048]{1,0:T(8,128)(2,1)S(1)} %all_gather.30, f32[2048]{0:T(1024)S(1)} %bitcast.216), kind=kOutput, calls=%fused_computation.43 | convolution fusion | flops 135069696 | bytes 1647104 | tf_op jit(solution)/shard_map/dot_general | solution.py:159
  30.9 3.5 %collective-permute-start = (bf16[2,256]{1,0:T(2,128)(2,1)S(1)}, bf16[2,256]{1,0:T(2,128)(2,1)S(1)}, u32[]{:S(2)}, u32[]{:S(2)}) collective-permute-start(bf16[2,256]{1,0:T(2,128)(2,1)S(1)} %slice.57), channel_id=1, source_target_pairs={{0,4},{4,8},{8,12},{12,16},{16,20},{20,24},{24,28},{1,5},{5,9},{9,... | collective-permute-start | bytes 3080 | tf_op jit(solution)/shard_map/ppermute | solution.py:17
  36.1 2.3 %fusion.17 = bf16[128,512]{1,0:T(8,128)(2,1)S(1)} fusion(bf16[2048,512]{1,0:T(8,128)(2,1)} %param.23, f32[128]{0:T(128)S(1)} %add_rsqrt_fusion.1, bf16[128,2048]{1,0:T(8,128)(2,1)S(1)} %all_gather.30, f32[2048]{0:T(1024)S(1)} %bitcast.217), kind=kOutput, calls=%fused_computation.36 | convolution fusion | flops 269352960 | bytes 2761216 | tf_op jit(solution)/shard_map/dot_general | solution.py:159
  40.5 27.0 %all-gather.4 = f32[8,2,256]{2,1,0:T(2,128)S(1)} all-gather(f32[1,2,256]{2,1,0:T(2,128)S(1)} %fusion.63), channel_id=5, replica_groups=mesh['sp'=8,'tp'=4] {'sp'}, dimensions={0}, use_global_device_ids=true | all-gather | bytes 18432 | tf_op jit(solution)/shard_map/all_gather | solution.py:22
  67.5 19.8 %all-reduce.2 = (f32[16]{0:T(128)S(1)}, f32[16]{0:T(128)S(1)}) all-reduce(f32[16]{0:T(128)S(1)} %dynamic-update-slice, f32[16]{0:T(128)S(1)} %dynamic-update-slice.1), channel_id=2, replica_groups=mesh['sp'=8,'tp'=4] {'sp'}, use_global_device_ids=true, to_apply=%add | all-reduce | flops 32 | bytes 256
  87.5 2.5 %fusion.50 = f32[128,2048]{1,0:T(8,128)} fusion(bf16[256,2048]{1,0:T(8,128)(2,1)} %param.30, f32[130,256]{1,0:T(8,128)S(1)} %maximum_convert_fusion, bf16[128,256]{1,0:T(8,128)(2,1)S(1)} %fusion.18, f32[256]{0:T(256)S(1)} %bitcast.230, f32[256]{0:T(256)S(1)} %bitcast.229, f32[256]{0:T(256)S(1)} %bitcast.228), kind=kOutput, calls=%fused_computation.85 | convolution fusion | flops 134479872 | bytes 2558976 | tf_op jit(solution)/shard_map/dot_general | solution.py:208
  90.1 12.7 %all-gather.7.cloned.1.call-done = f32[16,256,256]{2,1,0:T(8,128)} async-done(((f32[2,256,256]{2,1,0:T(8,128)}), f32[16,256,256]{2,1,0:T(8,128)}) %all-gather.7.cloned.1.call-update) | async-done | bytes 4194320 | tf_op jit(solution)/shard_map/all_gather | solution.py:22
  102.8 9.3 %while.5 = (s32[]{:T(128)}, f32[2]{0:T(128)S(1)}, f32[2,256,256]{2,1,0:T(8,128)S(1)}, f32[2,256]{1,0:T(2,128)S(1)}, s32[]{:T(128)}, /*index=5*/f32[8,2]{1,0:T(8,...) while((s32[]{:T(128)}, f32[2]{0:T(128)S(1)}, ...), condition=%wide.region_4.5_spmd.clone, body=%wide.region_3.4_spmd.clone.sunk | while | flops 657940 | bytes 1579278 | solution.py:31
  102.9 1.2 fusion.96
  104.3 1.2 fusion.96
  105.6 1.2 fusion.96
  106.9 1.2 fusion.96
  108.3 1.2 fusion.96
  109.6 1.2 fusion.96
  111.0 1.2 fusion.96
  113.2 5.7 %psum.7 = f32[128]{0:T(128)S(1)} all-reduce(f32[128]{0:T(128)S(1)} %get-tuple-element.276), channel_id=1, replica_groups=mesh['sp'=8,'tp'=4] {'tp'}, use_global_device_ids=true, to_apply=%region_7.8 | all-reduce | flops 128 | bytes 1024 | tf_op jit(solution)/shard_map/psum | solution.py:202
  118.9 2.5 %fusion.7 = bf16[128,2048]{1,0:T(8,128)(2,1)} fusion(f32[128,2048]{1,0:T(8,128)} %fusion.50, bf16[512,2048]{1,0:T(8,128)(2,1)S(1)} %copy-done, f32[128,512]{1,0:T(8,128)S(1)} %bitcast.211, bf16[128,512]{1,0:T(8,128)(2,1)S(1)} %fusion.14, f32[512]{0:T(512)S(1)} %convert_element_type.84, f32[128]{0:T(128)S(1)} %add_rsqrt_fusion), kind=kOutput, calls=%fused_computation.16 | convolution fusion | flops 269484032 | bytes 4065792 | tf_op jit(solution)/shard_map/dot_general | solution.py:209
  121.4 20.7 %reduce-scatter.2.cloned.1.call-done = bf16[32,2048]{1,0:T(8,128)(2,1)} async-done(((bf16[128,2048]{1,0:T(8,128)(2,1)}), bf16[32,2048]{1,0:T(8,128)(2,1)}) %reduce-scatter.2.cloned.1.call-update) | async-done | bytes 131088 | tf_op jit(solution)/shard_map/reduce_scatter | solution.py:206
  (83 shorter events, 7.8 us)
Async XLA Ops:
  6.5 112.4 %copy-start = (bf16[512,2048]{1,0:T(8,128)(2,1)S(1)}, bf16[512,2048]{1,0:T(8,128)(2,1)}, u32[]{:S(2)}) copy-start(bf16[512,2048]{1,0:T(8,128)(2,1)} %param.31) | copy-start | bytes 6291460
  6.5 96.3 %all-gather.7.cloned.1.call-start = ((), (), s32[]{:S(2)}) async-start(), calls=%async_computation.2 | async-start | bytes 4718592 | tf_op jit(solution)/shard_map/all_gather | solution.py:22
  23.2 2.7 %copy-start.1 = (bf16[2048,512]{1,0:T(8,128)(2,1)S(1)}, bf16[2048,512]{1,0:T(8,128)(2,1)}, u32[]{:S(2)}) copy-start(bf16[2048,512]{1,0:T(8,128)(2,1)} %param.25) | copy-start | bytes 6291460
  27.7 6.8 %copy-start.6 = (u32[32]{0:T(128)S(1)}, u32[32]{0:T(128)}, u32[]{:S(2)}) copy-start(u32[32]{0:T(128)} %constant.86) | copy-start | bytes 388
  27.7 114.4 %reduce-scatter.2.cloned.1.call-start = ((), (), s32[]{:S(2)}) async-start(), calls=%async_computation.1 | async-start | bytes 655360 | tf_op jit(solution)/shard_map/reduce_scatter | solution.py:206
  29.3 9.5 %copy-start.4 = (bf16[3,256]{1,0:T(4,128)(2,1)S(1)}, bf16[3,256]{1,0:T(4,128)(2,1)}, u32[]{:S(2)}) copy-start(bf16[3,256]{1,0:T(4,128)(2,1)} %param.22) | copy-start | bytes 4612
  30.9 56.6 %collective-permute-start = (bf16[2,256]{1,0:T(2,128)(2,1)S(1)}, bf16[2,256]{1,0:T(2,128)(2,1)S(1)}, u32[]{:S(2)}, u32[]{:S(2)}) collective-permute-start(bf16[2,256]{1,0:T(2,128)(2,1)S(1)} %slice.57), channel_id=1, source_target_pairs={{0,4},{4,8},{8,12},{12,16},{16,20},{20,24},{24,28},{1,5},{5,9},{9,... | collective-permute-start | bytes 3080 | tf_op jit(solution)/shard_map/ppermute | solution.py:17
  36.1 3.5 %copy-start.3 = (bf16[2048,256]{1,0:T(8,128)(2,1)S(1)}, bf16[2048,256]{1,0:T(8,128)(2,1)}, u32[]{:S(2)}) copy-start(bf16[2048,256]{1,0:T(8,128)(2,1)} %param.19) | copy-start | bytes 3145732
  38.4 1.6 %copy-start.2 = (bf16[2048,512]{1,0:T(8,128)(2,1)S(1)}, bf16[2048,512]{1,0:T(8,128)(2,1)}, u32[]{:S(2)}) copy-start(bf16[2048,512]{1,0:T(8,128)(2,1)} %param.26) | copy-start | bytes 6291460
  39.6 47.7 %copy-start.5 = (bf16[512]{0:T(512)(128)(2,1)S(1)}, bf16[512]{0:T(512)(128)(2,1)}, u32[]{:S(2)}) copy-start(bf16[512]{0:T(512)(128)(2,1)} %param.29) | copy-start | bytes 3076
Sparse Core Ops, SparseCore 0:
  27.8 74.9 all-gather.6
  121.6 20.4 reduce-scatter.1
where the time goes:
time: 150 us; the launch traced here: 149 us
  blocking collectives  66.7 us (44%)
  waiting for transfers between devices  33.4 us (22%)
  matrix products  17.4 us (12%)
  between operations  14.3 us (10%)
  other arithmetic  10.4 us (7%)
  starting transfers between devices  3.57 us (2%)
  local copies, waits for them, and re-layouts  2.92 us (2%)
    all_gather x1, blocking collectives, prefix(): pieces = jax.tree.map(lambda part: lax.all_gather(part, axis), value)  27 us
    reduce_scatter x1, waiting for transfers between devices, body(): lax.psum_scatter((jnp.dot(y_conv, conv_out_w, preferred_element_type=jnp....  20.7 us
    unnamed x1, blocking collectives  19.8 us
    all_gather x1, waiting for transfers between devices, prefix(): pieces = jax.tree.map(lambda part: lax.all_gather(part, axis), value)  12.7 us
    dot_general x8, matrix products, body(): jnp.dot(scaled, weight, preferred_element_type=jnp.float32)  9 us
    select_n x14, other arithmetic, prefix_step(): jnp.where(position < mine, new, old)  8.88 us
    all_gather x1, blocking collectives, body(): piece = lax.all_gather(tokens, 'tp', axis=1, tiled=True)  7.85 us
    all_gather x1, blocking collectives, body(): gain_piece = lax.all_gather(norm_gain, 'tp', axis=1, tiled=True)  6.32 us
  transfers between devices with their start and end apart: 3, of which 2 were waited for; matrix products, arithmetic and copies ran while one was open for 7% of the time, Pallas kernels for 0%

commit v1 on v0

--- a/solution.py
+++ b/solution.py
@@ -150,7 +150,9 @@
         outgate_w,
         gate_w.reshape(model, -1),
     )
-    piece = lax.all_gather(tokens, "tp", axis=1, tiled=True)
+    piece = jnp.concatenate(
+        lax.all_to_all(jnp.stack([tokens] * lax.axis_size("tp")), "tp", 0, 0), axis=1
+    )
     gain_piece = lax.all_gather(norm_gain, "tp", axis=1, tiled=True)
     wide = piece.astype(jnp.float32)
     scaled = (wide * gain_piece.astype(jnp.float32)).astype(jnp.bfloat16)

time: 150 us -> 154 us (1.027)
  waiting for transfers between devices: 33.4 us -> 23.9 us
  local copies, waits for them, and re-layouts: 2.92 us -> 11.2 us
  starting transfers between devices: 3.57 us -> 9.06 us
  blocking collectives: 66.7 us -> 61.6 us
  other arithmetic: 10.4 us -> 13.5 us
    all_gather x1, waiting for transfers between devices: 12.7 us -> 3.31 us  [prefix(): pieces = jax.tree.map(lambda part: lax.all_gather(part, axis), value)]
    all_gather x1 -> x0, blocking collectives: 7.85 us -> none  [body(): piece = lax.all_gather(tokens, 'tp', axis=1, tiled=True)]
    unnamed x19 -> x68, local copies, waits for them, and re-layouts: 1.15 us -> 6.67 us
    all_to_all x0 -> x1, starting transfers between devices: none -> 4.24 us  [body(): lax.all_to_all(jnp.stack([tokens] * lax.axis_size('tp')), 'tp', 0, 0)]
    all_gather x1, blocking collectives: 6.32 us -> 9.79 us  [body(): gain_piece = lax.all_gather(norm_gain, 'tp', axis=1, tiled=True)]
  transfers between devices with their start and end apart: 3 -> 4, of which waited for: 2 -> 2; matrix products, arithmetic and copies ran while one was open for 7% -> 14% of each run, Pallas kernels for 0% -> 0%
where the time goes in v1:
time: 154 us; the launch traced here: 153 us
  blocking collectives  61.6 us (40%)
  waiting for transfers between devices  23.9 us (16%)
  matrix products  18.4 us (12%)
  between operations  14.6 us (9%)
  other arithmetic  13.5 us (9%)
  local copies, waits for them, and re-layouts  11.2 us (7%)
  starting transfers between devices  9.06 us (6%)
    all_gather x1, blocking collectives, prefix(): pieces = jax.tree.map(lambda part: lax.all_gather(part, axis), value)  26.9 us
    reduce_scatter x1, waiting for transfers between devices, body(): lax.psum_scatter((jnp.dot(y_conv, conv_out_w, preferred_element_type=jnp....  20.6 us
    unnamed x1, blocking collectives  19.3 us
    all_gather x1, blocking collectives, body(): gain_piece = lax.all_gather(norm_gain, 'tp', axis=1, tiled=True)  9.79 us
    dot_general x8, matrix products, body(): jnp.dot(scaled, weight, preferred_element_type=jnp.float32)  8.93 us
    select_n x14, other arithmetic, prefix_step(): jnp.where(position < mine, new, old)  8.88 us
    unnamed x68, local copies, waits for them, and re-layouts  6.67 us
    psum x1, blocking collectives, body(): all_squares = lax.psum(own_squares, 'tp')  5.66 us
  transfers between devices with their start and end apart: 4, of which 2 were waited for; matrix products, arithmetic and copies ran while one was open for 14% of the time, Pallas kernels for 0%

profile of v1, /device:TPU:0, one launch (start us, length us, event | category | flops | bytes accessed | tf_op | source)
XLA Modules:
  0.0 152.7 jit_solution(1333496649463170908)
XLA Ops:
  8.6 4.2 %all-to-all-start = ((bf16[4,128,512]{1,2,0:T(8,128)(2,1)}), bf16[4,128,512]{1,2,0:T(8,128)(2,1)S(1)}, u32[]{:S(2)}, u32[]{:S(2)}) async-start(bf16[4,128,512]{1,2,0:T(8,128)(2,1)} %stack.2), calls=%async_computation | async-start | bytes 1048576 | tf_op jit(solution)/shard_map/all_to_all | solution.py:154
  12.8 9.8 %all_gather.27 = bf16[1,2048]{1,0:T(2,128)(2,1)S(1)} all-gather(bf16[1,512]{1,0:T(2,128)(2,1)} %param.18), channel_id=1, replica_groups=mesh['sp'=8,'tp'=4] {'tp'}, dimensions={1}, use_global_device_ids=true | all-gather | bytes 5120 | tf_op jit(solution)/shard_map/all_gather | solution.py:156
  26.9 2.2 %fusion.15 = bf16[128,512]{1,0:T(8,128)(2,1)S(1)} fusion(bf16[128,2048]{0,1:T(8,128)(2,1)S(1)} %fusion.21, bf16[2048,512]{1,0:T(8,128)(2,1)} %param.24, f32[128]{0:T(128)S(1)} %add_rsqrt_fusion.1), kind=kOutput, calls=%fused_computation.32 | convolution fusion | flops 268566528 | bytes 2753024 | tf_op jit(solution)/shard_map/dot_general | solution.py:161
  30.4 1.3 convolution_add_fusion.1
  31.8 1.3 convert_element_type.112
  33.1 1.3 dynamic-slice.10
  35.1 1.4 fusion.70
  37.0 1.2 dynamic-update-slice
  38.8 1.3 dynamic-update-slice.1
  40.1 1.8 %fusion.19 = bf16[128,256]{1,0:T(8,128)(2,1)S(1)} fusion(bf16[128,2048]{0,1:T(8,128)(2,1)S(1)} %fusion.21, bf16[2048,256]{1,0:T(8,128)(2,1)} %param.20, f32[128]{0:T(128)} %copy-done.13), kind=kOutput, calls=%fused_computation.40 | convolution fusion | flops 134283264 | bytes 1638912 | tf_op jit(solution)/shard_map/dot_general | solution.py:161
  42.0 1.6 %fusion.20 = bf16[128,256]{1,0:T(8,128)(2,1)S(1)} fusion(bf16[128,2048]{0,1:T(8,128)(2,1)S(1)} %fusion.21, bf16[2048,256]{1,0:T(8,128)(2,1)} %param.21, f32[128]{0:T(128)} %copy-done.13), kind=kOutput, calls=%fused_computation.41 | convolution fusion | flops 134283264 | bytes 1638912 | tf_op jit(solution)/shard_map/dot_general | solution.py:161
  44.3 4.8 %collective-permute-start = (bf16[2,256]{1,0:T(2,128)(2,1)}, bf16[2,256]{1,0:T(2,128)(2,1)}, u32[]{:S(2)}, u32[]{:S(2)}) collective-permute-start(bf16[2,256]{1,0:T(2,128)(2,1)} %slice.57), channel_id=1, source_target_pairs={{0,4},{4,8},{8,12},{12,16},{16,20},{20,24},{24,28},{1,5},{5,9},{9,... | collective-permute-start | bytes 3080 | tf_op jit(solution)/shard_map/ppermute | solution.py:17
  53.4 26.9 %all-gather.4 = f32[8,2,256]{2,1,0:T(2,128)S(1)} all-gather(f32[1,2,256]{2,1,0:T(2,128)S(1)} %fusion.54), channel_id=5, replica_groups=mesh['sp'=8,'tp'=4] {'sp'}, dimensions={0}, use_global_device_ids=true | all-gather | bytes 18432 | tf_op jit(solution)/shard_map/all_gather | solution.py:22
  80.3 19.3 %all-reduce.2 = (f32[16]{0:T(128)S(1)}, f32[16]{0:T(128)S(1)}) all-reduce(f32[16]{0:T(128)} %dynamic-update-slice, f32[16]{0:T(128)} %dynamic-update-slice.1), channel_id=2, replica_groups=mesh['sp'=8,'tp'=4] {'sp'}, use_global_device_ids=true, to_apply=%add | all-reduce | flops 32 | bytes 256
  100.6 2.6 %fusion.49 = f32[128,2048]{1,0:T(8,128)} fusion(bf16[256,2048]{1,0:T(8,128)(2,1)} %param.30, f32[130,256]{1,0:T(8,128)S(1)} %maximum_convert_fusion, bf16[128,256]{1,0:T(8,128)(2,1)} %fusion.18, f32[256]{0:T(256)} %bitcast.241, f32[256]{0:T(256)S(1)} %bitcast.240, f32[256]{0:T(256)S(1)} %bitcast.239), kind=kOutput, calls=%fused_computation.85 | convolution fusion | flops 134479872 | bytes 2558976 | tf_op jit(solution)/shard_map/dot_general | solution.py:210
  103.2 3.3 %all-gather.7.cloned.1.call-done = f32[16,256,256]{2,1,0:T(8,128)} async-done(((f32[2,256,256]{2,1,0:T(8,128)}), f32[16,256,256]{2,1,0:T(8,128)}) %all-gather.7.cloned.1.call-update) | async-done | bytes 4194320 | tf_op jit(solution)/shard_map/all_gather | solution.py:22
  106.6 9.4 %while.5 = (s32[]{:T(128)}, f32[2]{0:T(128)S(1)}, f32[2,256,256]{2,1,0:T(8,128)S(1)}, f32[2,256]{1,0:T(2,128)S(1)}, s32[]{:T(128)}, /*index=5*/f32[8,2]{1,0:T(8,...) while((s32[]{:T(128)}, f32[2]{0:T(128)S(1)}, ...), condition=%wide.region_4.5_spmd.clone, body=%wide.region_3.4_spmd.clone.sunk | while | flops 657940 | bytes 1579278 | solution.py:31
  106.7 1.2 fusion.95
  109.4 1.2 fusion.95
  110.7 1.2 fusion.95
  112.1 1.2 fusion.95
  117.0 5.7 %psum.7 = f32[128]{0:T(128)S(1)} all-reduce(f32[128]{0:T(128)S(1)} %get-tuple-element.278), channel_id=1, replica_groups=mesh['sp'=8,'tp'=4] {'tp'}, use_global_device_ids=true, to_apply=%region_7.8 | all-reduce | flops 128 | bytes 1024 | tf_op jit(solution)/shard_map/psum | solution.py:204
  122.7 2.5 %fusion.7 = bf16[128,2048]{1,0:T(8,128)(2,1)} fusion(f32[128,2048]{1,0:T(8,128)} %fusion.49, bf16[512,2048]{1,0:T(8,128)(2,1)S(1)} %copy-done, f32[128,512]{1,0:T(8,128)S(1)} %bitcast.229, bf16[128,512]{1,0:T(8,128)(2,1)S(1)} %fusion.14, f32[512]{0:T(512)S(1)} %copy-done.21, f32[128]{0:T(128)S(1)} %add_rsqrt_fusion), kind=kOutput, calls=%fused_computation.16 | convolution fusion | flops 269484032 | bytes 4065792 | tf_op jit(solution)/shard_map/dot_general | solution.py:211
  125.3 20.6 %reduce-scatter.2.cloned.1.call-done = bf16[32,2048]{1,0:T(8,128)(2,1)} async-done(((bf16[128,2048]{1,0:T(8,128)(2,1)}), bf16[32,2048]{1,0:T(8,128)(2,1)}) %reduce-scatter.2.cloned.1.call-update) | async-done | bytes 131088 | tf_op jit(solution)/shard_map/reduce_scatter | solution.py:208
  (137 shorter events, 19.9 us)
Async XLA Ops:
  6.5 116.2 %copy-start = (bf16[512,2048]{1,0:T(8,128)(2,1)S(1)}, bf16[512,2048]{1,0:T(8,128)(2,1)}, u32[]{:S(2)}) copy-start(bf16[512,2048]{1,0:T(8,128)(2,1)} %param.31) | copy-start | bytes 6291460
  8.6 15.6 %all-to-all-start = ((bf16[4,128,512]{1,2,0:T(8,128)(2,1)}), bf16[4,128,512]{1,2,0:T(8,128)(2,1)S(1)}, u32[]{:S(2)}, u32[]{:S(2)}) async-start(bf16[4,128,512]{1,2,0:T(8,128)(2,1)} %stack.2), calls=%async_computation | async-start | bytes 1048576 | tf_op jit(solution)/shard_map/all_to_all | solution.py:154
  12.8 93.7 %all-gather.7.cloned.1.call-start = ((), (), s32[]{:S(2)}) async-start(), calls=%async_computation.3 | async-start | bytes 4718592 | tf_op jit(solution)/shard_map/all_gather | solution.py:22
  26.2 4.2 %copy-start.19 = (f32[2,128]{1,0:T(2,128)}, f32[2,128]{1,0:T(2,128)S(1)}, u32[]{:S(2)}) copy-start(f32[2,128]{1,0:T(2,128)S(1)} %subtract_exponential_fusion.4) | copy-start | bytes 3076
  31.7 114.1 %reduce-scatter.2.cloned.1.call-start = ((), (), s32[]{:S(2)}) async-start(), calls=%async_computation.2 | async-start | bytes 655360 | tf_op jit(solution)/shard_map/reduce_scatter | solution.py:208
  40.1 8.9 %copy-start.2 = (bf16[2048,512]{1,0:T(8,128)(2,1)S(1)}, bf16[2048,512]{1,0:T(8,128)(2,1)}, u32[]{:S(2)}) copy-start(bf16[2048,512]{1,0:T(8,128)(2,1)} %param.23) | copy-start | bytes 6291460
  40.1 8.9 %copy-start.14 = (f32[128]{0:T(128)S(1)}, f32[128]{0:T(128)}, u32[]{:S(2)}) copy-start(f32[128]{0:T(128)} %copy-done.13) | copy-start | bytes 1540
  42.0 7.6 %copy-start.20 = (f32[2,128]{1,0:T(2,128)S(1)}, f32[2,128]{1,0:T(2,128)}, u32[]{:S(2)}) copy-start(f32[2,128]{1,0:T(2,128)} %copy-done.19) | copy-start | bytes 3076
  42.0 7.8 %copy-start.26 = (f32[2]{0:T(128)S(1)}, f32[2]{0:T(128)}, u32[]{:S(2)}) copy-start(f32[2]{0:T(128)} %get-tuple-element.236) | copy-start | bytes 28
  43.6 7.1 %copy-start.11 = (f32[2,128]{1,0:T(2,128)S(1)}, f32[2,128]{1,0:T(2,128)}, u32[]{:S(2)}) copy-start(f32[2,128]{1,0:T(2,128)} %copy-done.10) | copy-start | bytes 3076
  43.6 7.1 %copy-start.18 = (f32[2,128]{1,0:T(2,128)S(1)}, f32[2,128]{1,0:T(2,128)}, u32[]{:S(2)}) copy-start(f32[2,128]{1,0:T(2,128)} %copy-done.17) | copy-start | bytes 3076
  43.6 7.1 %copy-start.25 = (f32[2,128]{1,0:T(2,128)S(1)}, f32[2,128]{1,0:T(2,128)}, u32[]{:S(2)}) copy-start(f32[2,128]{1,0:T(2,128)} %copy-done.24) | copy-start | bytes 3076
  44.3 7.6 %copy-start.4 = (bf16[2048,256]{1,0:T(8,128)(2,1)S(1)}, bf16[2048,256]{1,0:T(8,128)(2,1)}, u32[]{:S(2)}) copy-start(bf16[2048,256]{1,0:T(8,128)(2,1)} %param.19) | copy-start | bytes 3145732
  44.3 55.4 %collective-permute-start = (bf16[2,256]{1,0:T(2,128)(2,1)}, bf16[2,256]{1,0:T(2,128)(2,1)}, u32[]{:S(2)}, u32[]{:S(2)}) collective-permute-start(bf16[2,256]{1,0:T(2,128)(2,1)} %slice.57), channel_id=1, source_target_pairs={{0,4},{4,8},{8,12},{12,16},{16,20},{20,24},{24,28},{1,5},{5,9},{9,... | collective-permute-start | bytes 3080 | tf_op jit(solution)/shard_map/ppermute | solution.py:17
  51.8 48.7 %copy-start.22 = (f32[1,256]{1,0:T(1,128)S(1)}, f32[1,256]{1,0:T(1,128)}, u32[]{:S(2)}) copy-start(f32[1,256]{1,0:T(1,128)} %get-tuple-element.271) | copy-start | bytes 3076
  51.9 48.7 %copy-start.23 = (f32[1,256]{1,0:T(1,128)S(1)}, f32[1,256]{1,0:T(1,128)}, u32[]{:S(2)}) copy-start(f32[1,256]{1,0:T(1,128)} %get-tuple-element.272) | copy-start | bytes 3076
  52.9 53.6 %copy-start.8 = (f32[2]{0:T(128)S(1)}, f32[2]{0:T(128)}, u32[]{:S(2)}) copy-start(f32[2]{0:T(128)} %custom-call) | copy-start | bytes 28
  52.9 53.6 %copy-start.9 = (f32[2,256]{1,0:T(2,128)S(1)}, f32[2,256]{1,0:T(2,128)}, u32[]{:S(2)}) copy-start(f32[2,256]{1,0:T(2,128)} %custom-call.2) | copy-start | bytes 6148
  106.5 9.4 %copy-start.6 = (bf16[128,512]{1,0:T(8,128)(2,1)S(1)}, bf16[128,512]{1,0:T(8,128)(2,1)}, u32[]{:S(2)}) copy-start(bf16[128,512]{1,0:T(8,128)(2,1)} %copy-done.5) | copy-start | bytes 393220
  106.5 9.6 %copy-start.12 = (f32[2,128]{1,0:T(2,128)S(1)}, f32[2,128]{1,0:T(2,128)}, u32[]{:S(2)}) copy-start(f32[2,128]{1,0:T(2,128)} %copy-done.10) | copy-start | bytes 3076
  106.5 9.6 %copy-start.16 = (f32[2,128]{1,0:T(2,128)S(1)}, f32[2,128]{1,0:T(2,128)}, u32[]{:S(2)}) copy-start(f32[2,128]{1,0:T(2,128)} %copy-done.15) | copy-start | bytes 3076
  106.5 9.6 %copy-start.29 = (f32[2,1,128]{2,1,0:T(1,128)S(1)}, f32[2,1,128]{2,1,0:T(1,128)}, u32[]{:S(2)}) copy-start(f32[2,1,128]{2,1,0:T(1,128)} %fusion.32) | copy-start | bytes 3076
  106.6 9.6 %copy-start.30 = (f32[2,128]{1,0:T(2,128)S(1)}, f32[2,128]{1,0:T(2,128)}, u32[]{:S(2)}) copy-start(f32[2,128]{1,0:T(2,128)} %get-tuple-element.276) | copy-start | bytes 3076
  115.9 6.8 %copy-start.21 = (f32[512]{0:T(512)S(1)}, f32[512]{0:T(512)}, u32[]{:S(2)}) copy-start(f32[512]{0:T(512)} %convert_element_type.112) | copy-start | bytes 6148
  (11 other events, 17.9 us)
Sparse Core Ops, SparseCore 0:
  31.8 74.6 all-gather.6
  125.4 20.4 reduce-scatter.1
